TPU v7x, 256 devices: a whole 4x4x8 slice. The times are simulated.
256 devices in a mesh: sp: 64 (over z, y, core), tp: 4 (over x).
Axes of the slice: x: 4, y: 4, z: 8, core: 2. Of those that a mesh axis runs over, the one named last changes fastest.
Arguments:
- memory_queries: bfloat16 [32768, 1024], P('sp', 'tp'), may hold values from -8 to 8
- memory_keys: bfloat16 [32768, 1024], P('sp', 'tp'), may hold values from -8 to 8
- memory_values: bfloat16 [32768, 1024], P('sp', 'tp'), may hold values from -6 to 6
- input_gate_logits: float32 [8, 32768], P('tp', 'sp'), may hold values from -64 to 160
- forget_gate_logits: float32 [8, 32768], P('tp', 'sp'), may hold values from -0.1 to 20
- extra_log_decay: float32 [8, 32768], P('tp', 'sp'), may hold values from -1.4 to 0
- residual: bfloat16 [32768, 2048], P(('sp', 'tp')), may hold values from -6 to 6
- cell_output_weight: bfloat16 [1024, 2048], P('tp', 'sp'), may hold values from -0.1875 to 0.1875
- expert_norm_gain: float32 [2048], replicated, may hold values from 0.1 to 1.9
- expert_gate_weight: bfloat16 [64, 2048, 3584], P('sp', None, 'tp'), may hold values from -0.125 to 0.125
- expert_up_weight: bfloat16 [64, 2048, 3584], P('sp', None, 'tp'), may hold values from -0.125 to 0.125
- expert_down_weight: bfloat16 [64, 3584, 2048], P('sp', 'tp'), may hold values from -0.09375 to 0.09375
- routed_expert_index: int32 [32768, 2], P('sp'), may hold values from 0 to 63, as said below
- routed_expert_weight: float32 [32768, 2], P(('sp', 'tp')), may hold values from 0.1 to 1
Outputs:
- layer_out: bfloat16 [32768, 2048], P(('sp', 'tp'))
Inputs may be any that keep to these rules, and one draw needn't show every extreme that they name: `routed_expert_index`: each row names 2 different experts. In each aligned block of 128 rows (the rows of one device after the cell) no expert is named more than 5 times, and one expert is named exactly 5 times in every block.
All inputs are finite; a program needn't handle non-finite values.
Results may differ from a plain program's by a relative error of at most 0.013.
Values may be sent and summed in bfloat16 or wider, within the bound.
No kernel may reach another device: no remote copies, remote signals or barrier semaphores. Data moves between devices by JAX's collectives and lax.ppermute only.
A program may use at most 128 MiB of HBM per device.

v0:
```python
import jax
import jax.numpy as jnp
from jax import lax
from jax.sharding import Mesh
from jax.sharding import PartitionSpec as P

SP = ("sp_0", "sp_1", "sp_2")
SP_TP = ("sp_0", "sp_1", "sp_2", "tp")
lowest = -1e30
epsilon = 1e-06


def neutral_like(x, identity):
    return jax.tree.map(
        lambda a, e: jnp.broadcast_to(jnp.asarray(e, a.dtype), a.shape), x, identity
    )


def collected_together(x, axis):
    leaves = jax.tree.leaves(x)
    turns = sorted(range(len(leaves)), key=lambda k: -leaves[k].size)
    width = (1, *leaves[turns[0]].shape)[-1]
    lines = [
        jnp.pad(leaves[k].reshape(-1), (0, -leaves[k].size % width)).reshape(-1, width)
        for k in turns
    ]
    both, at, found = (lax.all_gather(jnp.concatenate(lines), axis), 0, {})
    for k, line in zip(turns, lines):
        piece = both[:, at : at + len(line)].reshape(len(both), -1)
        found[k] = piece[:, : leaves[k].size].reshape(-1, *leaves[k].shape)
        at += len(line)
    numbers = iter(range(len(leaves)))
    return jax.tree.map(lambda _: found[next(numbers)], x)


def prefix_by_axis(x, axes, combine, identity):
    before = start = neutral_like(x, identity)
    running = x
    for axis in reversed(axes):
        length, place = (lax.axis_size(axis), lax.axis_index(axis))
        pieces = collected_together(running, axis)
        inside, running = (start, start)
        for k in range(length):
            passed = k < place
            running = combine(running, jax.tree.map(lambda part: part[k], pieces))
            inside = jax.tree.map(lambda new, old: jnp.where(passed, new, old), running, inside)
        before = combine(inside, before)
    return before


def from_everyone(x, axis):
    copies = jnp.broadcast_to(x, (lax.axis_size(axis), *x.shape))
    return lax.all_to_all(copies, axis, split_axis=0, concat_axis=0, tiled=True)


def laid_out(pieces, dim):
    dims = list(pieces.shape[1:])
    dims[dim] *= pieces.shape[0]
    return jnp.moveaxis(pieces, 0, dim).reshape(dims)


def gathered_copies(x, axis, dim):
    pieces = from_everyone(x, axis)
    return laid_out(pieces, dim)


def in_blocks(x, dim, length):
    before, after = (x.shape[:dim], x.shape[dim + 1 :])
    return jnp.moveaxis(x.reshape(*before, length, -1, *after), dim, 0)


def sent_and_summed(x, axis, dim):
    length = lax.axis_size(axis)
    pieces = lax.all_to_all(in_blocks(x, dim, length), axis, 0, 0, tiled=True)
    return jnp.sum(pieces.astype(jnp.float32), axis=0)


def block_pass(memory, inputs):
    state_mat, state_norm, state_max = memory
    queries, keys_blk, values_blk, gate_in, forget_log_value = inputs
    length = gate_in.shape[-1]
    running = jnp.cumsum(forget_log_value, axis=-1)
    causal = jnp.arange(length)[:, None] >= jnp.arange(length)[None, :]
    exponent = running[:, :, None] - running[:, None, :] + gate_in[:, None, :]
    exponent = jnp.where(causal[None], exponent, -jnp.inf)
    carried = running + state_max[:, None]
    row_max = jnp.maximum(carried, jnp.max(exponent, axis=-1))
    decays = jnp.exp(exponent - row_max[:, :, None])
    carry_scale = jnp.exp(carried - row_max)
    dispatch_affinity = jnp.einsum("htk,hsk->hts", queries, keys_blk) * decays
    numerator = carry_scale[:, :, None] * jnp.einsum("hvk,htk->htv", state_mat, queries)
    numerator = numerator + jnp.einsum("hts,hsv->htv", dispatch_affinity, values_blk)
    denominator = carry_scale * jnp.einsum("hk,htk->ht", state_norm, queries) + jnp.sum(
        dispatch_affinity, axis=-1
    )
    final_log = running[:, -1]
    log_prev = final_log + state_max
    log_keep = final_log[:, None] - running + gate_in
    new_max = jnp.maximum(log_prev, jnp.max(log_keep, axis=-1))
    prev_scale = jnp.exp(log_prev - new_max)
    retain = jnp.exp(log_keep - new_max[:, None])
    new_mat = prev_scale[:, None, None] * state_mat + jnp.einsum(
        "hsv,hsk->hvk", retain[:, :, None] * values_blk, keys_blk
    )
    new_norm = prev_scale[:, None] * state_norm + jnp.einsum("hs,hsk->hk", retain, keys_blk)
    return ((new_mat, new_norm, new_max), (numerator, denominator, row_max))


def join_states(earlier, later):
    early_log, early_mat, early_norm, early_max = earlier
    late_log, late_mat, late_norm, late_max = later
    joined_max = jnp.maximum(early_max + late_log, late_max)
    early_scale = jnp.exp(early_max + late_log - joined_max)
    late_scale = jnp.exp(late_max - joined_max)
    joined_mat = early_scale[:, None, None] * early_mat + late_scale[:, None, None] * late_mat
    joined_norm = early_scale[:, None] * early_norm + late_scale[:, None] * late_norm
    return (early_log + late_log, joined_mat, joined_norm, joined_max)


def matrix_memory_step(
    memory_queries,
    memory_keys,
    memory_values,
    input_gate_logits,
    forget_gate_logits,
    extra_log_decay,
):
    tokens_here, channels = memory_queries.shape
    heads_here = input_gate_logits.shape[0]
    head_dim = channels // heads_here

    def heads_first(tensor):
        return jnp.transpose(
            tensor.astype(jnp.float32).reshape(tokens_here, heads_here, head_dim), (1, 0, 2)
        )

    queries = heads_first(memory_queries) * head_dim ** (-0.5)
    forget_log_value = jax.nn.log_sigmoid(forget_gate_logits) + extra_log_decay
    block_size = min(tokens_here, 256)
    block_count = tokens_here // block_size

    def split_blocks(tensor):
        return jnp.moveaxis(
            tensor.reshape((heads_here, block_count, block_size) + tensor.shape[2:]), 1, 0
        )

    def join_blocks(tensor):
        return jnp.moveaxis(tensor, 0, 1).reshape((heads_here, tokens_here) + tensor.shape[3:])

    empty_state = (
        jnp.zeros((heads_here, head_dim, head_dim), jnp.float32),
        jnp.zeros((heads_here, head_dim), jnp.float32),
        jnp.full((heads_here,), lowest, jnp.float32),
    )
    members = (
        queries,
        heads_first(memory_keys),
        heads_first(memory_values),
        input_gate_logits,
        forget_log_value,
    )
    end_state, pieces = lax.scan(
        block_pass, empty_state, tuple((split_blocks(member) for member in members))
    )
    numerator, denominator, row_max = (join_blocks(member) for member in pieces)
    running = jnp.cumsum(forget_log_value, axis=-1)
    identity = (jnp.zeros((heads_here,), jnp.float32),) + empty_state
    incoming = prefix_by_axis((running[:, -1],) + tuple(end_state), SP, join_states, identity)
    prior_mat, prior_norm, prior_max = incoming[1:]
    reached = running + prior_max[:, None]
    joined = jnp.maximum(row_max, reached)
    local_scale = jnp.exp(row_max - joined)
    carry_scale = jnp.exp(reached - joined)
    numerator = local_scale[:, :, None] * numerator + carry_scale[:, :, None] * jnp.einsum(
        "hvk,htk->htv", prior_mat, queries
    )
    denominator = local_scale * denominator + carry_scale * jnp.einsum(
        "hk,htk->ht", prior_norm, queries
    )
    guarded = jnp.maximum(jnp.abs(denominator), jnp.exp(-joined))
    return ((numerator / guarded[:, :, None]).astype(jnp.bfloat16), heads_here, head_dim)


def slot_index(ids, experts, capacity):
    flat_ids = ids.reshape(-1)
    matches = (flat_ids[:, None] == jnp.arange(experts, dtype=jnp.int32)[None, :]).astype(jnp.int32)
    before = jnp.cumsum(matches, axis=0) - matches
    return flat_ids * capacity + jnp.sum(before * matches, axis=1)


def local(
    memory_queries,
    memory_keys,
    memory_values,
    input_gate_logits,
    forget_gate_logits,
    extra_log_decay,
    residual,
    cell_output_weight,
    expert_norm_gain,
    expert_gate_weight,
    expert_up_weight,
    expert_down_weight,
    routed_expert_index,
    routed_expert_weight,
):
    hidden, heads_here, head_dim = matrix_memory_step(
        memory_queries,
        memory_keys,
        memory_values,
        input_gate_logits,
        forget_gate_logits,
        extra_log_decay,
    )
    weight_piece = gathered_copies(cell_output_weight, SP, 1)
    shaped = weight_piece.reshape(heads_here, head_dim, weight_piece.shape[1])
    partial_rows = jnp.einsum(
        "htd,hdc->tc", hidden, shaped, preferred_element_type=jnp.float32
    ).astype(jnp.bfloat16)
    projected = sent_and_summed(partial_rows.astype(jnp.float32).astype(jnp.bfloat16), "tp", 0)
    mixed_rows = (residual.astype(jnp.float32) + projected).astype(jnp.bfloat16)
    mixed_wide = mixed_rows.astype(jnp.float32)
    norm_scale = lax.rsqrt(jnp.mean(mixed_wide * mixed_wide, axis=-1, keepdims=True) + epsilon)
    normed = (mixed_wide * norm_scale * expert_norm_gain).astype(jnp.bfloat16)
    sp_size = lax.axis_size(SP)
    row_count, model_width = residual.shape
    top_count = routed_expert_index.shape[1]
    experts = sp_size * expert_gate_weight.shape[0]
    assigned = row_count * top_count
    capacity = max(2, assigned * 5 // (4 * experts))
    own_ids = lax.dynamic_slice_in_dim(
        routed_expert_index, lax.axis_index("tp") * row_count, row_count, 0
    )
    own_slots = slot_index(own_ids, experts, capacity)
    zero_row = jnp.zeros((1, model_width), jnp.bfloat16)
    padded = jnp.concatenate([normed, zero_row], axis=0)
    slot_table = jnp.full((experts * capacity,), row_count, jnp.int32)
    slot_table = slot_table.at[own_slots].set(jnp.arange(assigned, dtype=jnp.int32) // top_count)
    arrived = lax.all_gather(
        lax.all_to_all(
            padded[slot_table.reshape(experts, 1, capacity)],
            SP,
            split_axis=0,
            concat_axis=0,
            tiled=True,
        ),
        "tp",
        axis=1,
        tiled=True,
    )
    sources, owners, slot_span, width_in = arrived.shape
    flat_rows = arrived.reshape(-1, width_in)
    gate_pre = jnp.dot(flat_rows, expert_gate_weight[0], preferred_element_type=jnp.float32)
    up_pre = jnp.dot(flat_rows, expert_up_weight[0], preferred_element_type=jnp.float32)
    hidden_act = (jax.nn.silu(gate_pre) * up_pre).astype(jnp.bfloat16)
    group_term = jnp.dot(hidden_act, expert_down_weight[0], preferred_element_type=jnp.float32)
    group_term = lax.optimization_barrier(group_term.astype(jnp.bfloat16)).astype(jnp.float32)
    summed = lax.psum_scatter(
        group_term.reshape(sources, owners, slot_span, width_in).astype(jnp.bfloat16),
        "tp",
        scatter_dimension=1,
        tiled=True,
    )
    returned = lax.all_to_all(summed, SP, split_axis=0, concat_axis=0, tiled=True)
    picked = returned.reshape(experts * capacity, model_width)[own_slots]
    picked = picked.reshape(row_count, top_count, model_width).astype(jnp.float32)
    routed_sum = jnp.sum(picked * routed_expert_weight[:, :, None], axis=1)
    return (mixed_wide + routed_sum).astype(jnp.bfloat16)


def solution(mesh):
    finer = Mesh(mesh.devices.reshape(8, 4, 2, mesh.shape["tp"]), ("sp_0", "sp_1", "sp_2", "tp"))
    placed = (
        P(SP, "tp"),
        P(SP, "tp"),
        P(SP, "tp"),
        P("tp", SP),
        P("tp", SP),
        P("tp", SP),
        P(SP_TP, None),
        P("tp", SP),
        P(),
        P(SP, None, "tp"),
        P(SP, None, "tp"),
        P(SP, "tp", None),
        P(SP, None),
        P(SP_TP, None),
    )
    return jax.shard_map(
        local, mesh=finer, in_specs=placed, out_specs=P(SP_TP, None), check_vma=False
    )
```

profile of v0, /device:TPU:8, one launch (start us, length us, event | category | flops | bytes accessed | tf_op | source)
XLA Modules:
  0.0 450.7 jit_solution(14113384938206479818)
XLA Ops:
  9.8 7.3 %while.21 = (s32[]{:T(128)}, f32[2,128,128]{2,1,0:T(8,128)S(1)}, f32[2,128]{1,0:T(2,128)S(1)}, f32[2]{0:T(128)S(1)}, f32[2,2,256,128]{3,2,0,1:T(8,128)S(1)}, /*i...) while((s32[]{:T(128)}, f32[2,128,128]{2,1,0:T(8,128)S(1)}, ...), condition=%wide.region_6.7_spmd.clone, body=%wide.region_0.6_spmd.clone.sunk | while | flops 102833424 | bytes 3183522 | solution.py:162
  20.7 13.0 %all-gather.4 = f32[4,260,128]{2,1,0:T(8,128)S(1)} all-gather(f32[1,260,128]{2,1,0:T(8,128)S(1)} %maximum_bitcast_fusion.1), channel_id=3, replica_groups=mesh['sp_0'=8,'sp_1'=4,'sp_2'=2,'tp'=4] {'sp_1'}, dimensions={0}, use_global_device_ids=true | all-gather | bytes 665600 | tf_op jit(solution)/shard_map/all_gather | solution.py:27
  36.2 12.4 %all-to-all-start = ((bf16[64,256,32]{1,2,0:T(8,128)(2,1)}), bf16[64,256,32]{1,2,0:T(8,128)(2,1)S(1)}, u32[]{:S(2)}, u32[]{:S(2)}) async-start(bf16[64,256,32]{1,2,0:T(8,128)(2,1)} %broadcast_in_dim.50), calls=%async_computation | async-start | bytes 2097152 | tf_op jit(solution)/shard_map/all_to_all | solution.py:53
  50.1 36.4 %all-gather.11.cloned.1.call-done = f32[8,260,128]{2,1,0:T(8,128)} async-done(((f32[1,260,128]{2,1,0:T(8,128)}), f32[8,260,128]{2,1,0:T(8,128)}) %all-gather.11.cloned.1.call-update) | async-done | bytes 1064976 | tf_op jit(solution)/shard_map/all_gather | solution.py:27
  88.9 2.1 fusion.349
  91.3 4.1 bitcast_convert_fusion
  95.3 4.4 all-to-all-start.1
  103.8 21.2 %all-to-all-done.1 = bf16[4,128,2048]{2,1,0:T(8,128)(2,1)S(1)} async-done(((bf16[4,128,2048]{2,1,0:T(8,128)(2,1)}), bf16[4,128,2048]{2,1,0:T(8,128)(2,1)S(1)}, u32[]{:S(2)}, u32[]{:S(2)}) %all-to-all-start.1) | async-done | bytes 2097184 | tf_op jit(solution)/shard_map/all_to_all | solution.py:74
  126.6 2.4 gather_fusion
  129.6 60.1 %all_to_all.20 = bf16[64,1,5,2048]{3,2,1,0:T(8,128)(2,1)S(1)} all-to-all(bf16[64,1,5,2048]{3,2,1,0:T(8,128)(2,1)S(1)} %bitcast.677), channel_id=1, replica_groups=mesh['sp_0'=8,'sp_1'=4,'sp_2'=2,'tp'=4] {'sp_0','sp_1','sp_2'}, dimensions={0} | all-to-all | bytes 2621440 | tf_op jit(solution)/shard_map/all_to_all | solution.py:240
  191.7 53.9 %all-gather.9.cloned.1.call-done = bf16[64,4,5,2048]{3,0,2,1:T(8,128)(2,1)} async-done(((bf16[64,1,5,2048]{3,0,2,1:T(8,128)(2,1)}), bf16[64,4,5,2048]{3,0,2,1:T(8,128)(2,1)}) %all-gather.9.cloned.1.call-update) | async-done | bytes 5242896 | tf_op jit(solution)/shard_map/all_gather | solution.py:239
  245.6 8.9 %copy.125 = bf16[64,4,5,2048]{3,2,1,0:T(8,128)(2,1)} copy(bf16[64,4,5,2048]{3,0,2,1:T(8,128)(2,1)} %all-gather.9.cloned.1.call-done) | data formatting | bytes 10485760 | tf_op jit(solution)/shard_map/all_gather | solution.py:239
  254.4 10.0 %reshape.2836 = bf16[1280,2048]{1,0:T(8,128)(2,1)} reshape(bf16[64,4,5,2048]{3,2,1,0:T(8,128)(2,1)} %copy.125) | data formatting | bytes 10485760 | tf_op jit(solution)/shard_map/reshape | solution.py:252
  264.5 9.9 %fusion.36 = f32[1280,896]{1,0:T(8,128)} fusion(bf16[1280,2048]{1,0:T(8,128)(2,1)} %reshape.2836, bf16[1,2048,896]{2,1,0:T(8,128)(2,1)} %param.25), kind=kOutput, calls=%fused_computation.67 | convolution fusion | flops 4697620480 | bytes 13500416 | tf_op jit(solution)/shard_map/dot_general | solution.py:253
  274.4 17.5 %convolution_convert_fusion = bf16[1280,2048]{1,0:T(8,128)(2,1)} fusion(bf16[1,896,2048]{2,1,0:T(8,128)(2,1)} %param.27, f32[1280,896]{1,0:T(8,128)} %fusion.36, bf16[1280,2048]{1,0:T(8,128)(2,1)} %reshape.2836, bf16[1,2048,896]{2,1,0:T(8,128)(2,1)} %param.26), kind=kOutput, calls=%fused_computation.61 | convolution fusion | flops 9404743680 | bytes 22413312 | tf_op jit(solution)/shard_map/dot_general | solution.py:256
  291.9 9.8 %convert_element_type.74 = bf16[64,4,5,2048]{3,2,1,0:T(8,128)(2,1)} reshape(bf16[1280,2048]{1,0:T(8,128)(2,1)} %convolution_convert_fusion) | data formatting | bytes 10485760 | tf_op jit(solution)/shard_map/convert_element_type | solution.py:259
  301.6 9.2 %copy.126 = bf16[64,4,5,2048]{3,0,2,1:T(8,128)(2,1)} copy(bf16[64,4,5,2048]{3,2,1,0:T(8,128)(2,1)} %convert_element_type.74) | data formatting | bytes 10485760 | tf_op jit(solution)/shard_map/convert_element_type | solution.py:259
  310.9 58.6 %reduce-scatter.2.cloned.1.call-done = bf16[64,1,5,2048]{3,0,2,1:T(8,128)(2,1)} async-done(((bf16[64,4,5,2048]{3,0,2,1:T(8,128)(2,1)}), bf16[64,1,5,2048]{3,0,2,1:T(8,128)(2,1)}) %reduce-scatter.2.cloned.1.call-update) | async-done | bytes 1310736 | tf_op jit(solution)/shard_map/reduce_scatter | solution.py:258
  369.5 3.4 copy.127
  372.9 10.6 %all-to-all-start.3 = ((bf16[64,1,5,2048]{3,2,1,0:T(8,128)(2,1)}), bf16[64,1,5,2048]{3,2,1,0:T(8,128)(2,1)S(1)}, u32[]{:S(2)}, u32[]{:S(2)}) async-start(bf16[64,1,5,2048]{3,2,1,0:T(8,128)(2,1)} %copy.127), calls=%async_computation.4 | async-start | bytes 4194304 | tf_op jit(solution)/shard_map/all_to_all | solution.py:264
  383.6 51.1 %all-to-all-done.3 = bf16[64,1,5,2048]{3,2,1,0:T(8,128)(2,1)S(1)} async-done(((bf16[64,1,5,2048]{3,2,1,0:T(8,128)(2,1)}), bf16[64,1,5,2048]{3,2,1,0:T(8,128)(2,1)S(1)}, u32[]{:S(2)}, u32[]{:S(2)}) %all-to-all-start.3) | async-done | bytes 1310752 | tf_op jit(solution)/shard_map/all_to_all | solution.py:264
  435.3 2.3 gather_fusion.1
  437.6 2.4 reshape.2838
  440.1 3.2 multiply_reduce_fusion
  (178 shorter events, 29.8 us)
Async XLA Ops:
  6.5 2.8 copy-start.3
  6.5 3.1 copy-start.8
  6.5 3.1 copy-start.7
  6.5 3.2 copy-start.4
  6.5 80.0 %all-gather.11.cloned.1.call-start = ((), (), s32[]{:S(2)}) async-start(), calls=%async_computation.7 | async-start | bytes 1216512 | tf_op jit(solution)/shard_map/all_gather | solution.py:27
  9.7 25.2 %copy-start.5 = (bf16[256,32]{0,1:T(8,128)(2,1)S(1)}, bf16[256,32]{0,1:T(8,128)(2,1)}, u32[]{:S(2)}) copy-start(bf16[256,32]{0,1:T(8,128)(2,1)} %param.23) | copy-start | bytes 49156
  20.4 13.4 %copy-start.12 = (f32[2]{0:T(128)}, f32[2]{0:T(128)S(1)}, u32[]{:S(2)}) copy-start(f32[2]{0:T(128)S(1)} %fusion.337) | copy-start | bytes 28
  33.8 2.3 copy-start.9
  33.8 2.3 copy-start.10
  33.8 53.6 %copy-start.13 = (f32[2]{0:T(128)}, f32[2]{0:T(128)S(1)}, u32[]{:S(2)}) copy-start(f32[2]{0:T(128)S(1)} %fusion.333) | copy-start | bytes 28
  36.2 54.8 %all-to-all-start = ((bf16[64,256,32]{1,2,0:T(8,128)(2,1)}), bf16[64,256,32]{1,2,0:T(8,128)(2,1)S(1)}, u32[]{:S(2)}, u32[]{:S(2)}) async-start(bf16[64,256,32]{1,2,0:T(8,128)(2,1)} %broadcast_in_dim.50), calls=%async_computation | async-start | bytes 2097152 | tf_op jit(solution)/shard_map/all_to_all | solution.py:53
  88.4 2.8 copy-start.14
  95.3 30.1 %copy-start.2 = (bf16[128,2048]{1,0:T(8,128)(2,1)S(1)}, bf16[128,2048]{1,0:T(8,128)(2,1)}, u32[]{:S(2)}) copy-start(bf16[128,2048]{1,0:T(8,128)(2,1)} %param.22) | copy-start | bytes 1572868
  95.3 29.7 %all-to-all-start.1 = ((bf16[4,128,2048]{2,1,0:T(8,128)(2,1)}), bf16[4,128,2048]{2,1,0:T(8,128)(2,1)S(1)}, u32[]{:S(2)}, u32[]{:S(2)}) async-start(bf16[4,128,2048]{2,1,0:T(8,128)(2,1)} %bitcast.682), calls=%async_computation.1 | async-start | bytes 4194304 | tf_op jit(solution)/shard_map/all_to_all | solution.py:74
  99.8 26.0 %copy-start.6 = (f32[2048]{0:T(1024)S(1)}, f32[2048]{0:T(1024)}, u32[]{:S(2)}) copy-start(f32[2048]{0:T(1024)} %param.24) | copy-start | bytes 24580
  99.8 145.8 %all-gather.9.cloned.1.call-start = ((), (), s32[]{:S(2)}) async-start(), calls=%async_computation.5 | async-start | bytes 6553600 | tf_op jit(solution)/shard_map/all_gather | solution.py:239
  125.7 0.8 copy-start
  191.6 177.9 %reduce-scatter.2.cloned.1.call-start = ((), (), s32[]{:S(2)}) async-start(), calls=%async_computation.6 | async-start | bytes 6553600 | tf_op jit(solution)/shard_map/reduce_scatter | solution.py:258
  310.9 72.6 %copy-start.11 = (f32[128,2]{0,1:T(2,128)S(1)}, f32[128,2]{0,1:T(2,128)}, u32[]{:S(2)}) copy-start(f32[128,2]{0,1:T(2,128)} %param.29) | copy-start | bytes 3076
  372.9 61.8 %all-to-all-start.3 = ((bf16[64,1,5,2048]{3,2,1,0:T(8,128)(2,1)}), bf16[64,1,5,2048]{3,2,1,0:T(8,128)(2,1)S(1)}, u32[]{:S(2)}, u32[]{:S(2)}) async-start(bf16[64,1,5,2048]{3,2,1,0:T(8,128)(2,1)} %copy.127), calls=%async_computation.4 | async-start | bytes 4194304 | tf_op jit(solution)/shard_map/all_to_all | solution.py:264
  437.6 5.6 %copy-start.1 = (bf16[128,2048]{1,0:T(8,128)(2,1)S(1)}, bf16[128,2048]{1,0:T(8,128)(2,1)}, u32[]{:S(2)}) copy-start(bf16[128,2048]{1,0:T(8,128)(2,1)} %copy-done) | copy-start | bytes 1572868
Sparse Core Ops, SparseCore 0:
  35.1 51.3 all-gather.10
  191.7 53.7 all-gather.8
  311.0 58.4 reduce-scatter.1
where the time goes:
time: 452 us; the launch traced here: 451 us
  waiting for transfers between devices  221 us (49%)
  blocking collectives  75.1 us (17%)
  local copies, waits for them, and re-layouts  64.7 us (14%)
  matrix products  34.4 us (8%)
  starting transfers between devices  27.4 us (6%)
  other arithmetic  13.7 us (3%)
  between operations  13.7 us (3%)
    all_to_all x1, blocking collectives, local(): lax.all_to_all(padded[slot_table.reshape(experts, 1, capacity)], SP, spli...  60.1 us
    reduce_scatter x1, waiting for transfers between devices, local(): lax.psum_scatter(group_term.reshape(sources, owners, slot_span, width_in)...  58.6 us
    all_gather x1, waiting for transfers between devices, local(): lax.all_gather(lax.all_to_all(padded[slot_table.reshape(experts, 1, capac...  53.9 us
    all_to_all x1, waiting for transfers between devices, local(): lax.all_to_all(summed, SP, split_axis=0, concat_axis=0, tiled=True)  51.1 us
    all_gather x1, waiting for transfers between devices, collected_together(): both, at, found = (lax.all_gather(jnp.concatenate(lines), axis), 0, {})  36.4 us
    all_to_all x1, waiting for transfers between devices, sent_and_summed(): pieces = lax.all_to_all(in_blocks(x, dim, length), axis, 0, 0, tiled=True)  21.2 us
    convert_element_type x2, local copies, waits for them, and re-layouts, local(): group_term.reshape(sources, owners, slot_span, width_in)  19 us
    dot_general x1, matrix products, local(): jnp.dot(hidden_act, expert_down_weight[0], preferred_element_type=jnp.flo...  17.5 us
  transfers between devices with their start and end apart: 6, of which 5 were waited for; matrix products, arithmetic and copies ran while one was open for 2% of the time, Pallas kernels for 0%

commit v1 on v0

--- a/solution.py
+++ b/solution.py
@@ -8,6 +8,28 @@
 SP_TP = ("sp_0", "sp_1", "sp_2", "tp")
 lowest = -1e30
 epsilon = 1e-06
+
+
+def in_order(parts, dim):
+    parts = jnp.moveaxis(parts, 0, dim)
+    lengths = parts.shape
+    return parts.reshape(*lengths[:dim], lengths[dim] * lengths[dim + 1], *lengths[dim + 2 :])
+
+
+def gather_around(x, axis, dim):
+    count = lax.axis_size(axis)
+    pairs = [(i, (i + 1) % count) for i in range(count)]
+    back = [(b, a) for a, b in pairs]
+    lower, upper = ([], [])
+    for hop in range(count - 1):
+        if hop % 2 == 0:
+            lower.append(lax.ppermute(lower[-1] if lower else x, axis, pairs))
+        else:
+            upper.append(lax.ppermute(upper[-1] if upper else x, axis, back))
+    blocks = jnp.stack([*lower[::-1], x, *upper])
+    shift = lax.axis_index(axis) - len(lower)
+    blocks = blocks[(jnp.arange(count) - shift) % count]
+    return in_order(blocks, dim)
 
 
 def neutral_like(x, identity):
@@ -236,7 +258,7 @@
     padded = jnp.concatenate([normed, zero_row], axis=0)
     slot_table = jnp.full((experts * capacity,), row_count, jnp.int32)
     slot_table = slot_table.at[own_slots].set(jnp.arange(assigned, dtype=jnp.int32) // top_count)
-    arrived = lax.all_gather(
+    arrived = gather_around(
         lax.all_to_all(
             padded[slot_table.reshape(experts, 1, capacity)],
             SP,
@@ -245,8 +267,7 @@
             tiled=True,
         ),
         "tp",
-        axis=1,
-        tiled=True,
+        1,
     )
     sources, owners, slot_span, width_in = arrived.shape
     flat_rows = arrived.reshape(-1, width_in)

time: 452 us -> 489 us (1.082); the launches traced: 451 us -> 479 us
  local copies, waits for them, and re-layouts: 64.7 us -> 78 us
  blocking collectives: 75.1 us -> 84.9 us
    all_gather x1 -> x0, waiting for transfers between devices: 53.9 us -> none  [local(): lax.all_gather(lax.all_to_all(padded[slot_table.reshape(experts, 1, capac...]
    ppermute x0 -> x3, waiting for transfers between devices: none -> 53.8 us  [the longest x2 53.8 us: gather_around(): lower.append(lax.ppermute(lower[-1] if lower else x, axis, pairs))]
    reshape x3 -> x2, local copies, waits for them, and re-layouts: 10 us -> 0.03 us  [the longest x1 10 us: local(): flat_rows = arrived.reshape(-1, width_in)]
    another operation x6 -> x7, local copies, waits for them, and re-layouts: 0.4 us -> 10.4 us  [the longest x1 10 us: local(): flat_rows = arrived.reshape(-1, width_in)]
    all_to_all x1, blocking collectives: 60.1 us -> 69.8 us  [local(): lax.all_to_all(padded[slot_table.reshape(experts, 1, capacity)], SP, spli...]
    all_gather x1 -> x0, local copies, waits for them, and re-layouts: 8.89 us -> none  [local(): lax.all_gather(lax.all_to_all(padded[slot_table.reshape(experts, 1, capac...]
    transpose x0 -> x1, local copies, waits for them, and re-layouts: none -> 8.27 us  [in_order(): parts = jnp.moveaxis(parts, 0, dim)]
    gather x0 -> x1, local copies, waits for them, and re-layouts: none -> 8.01 us  [gather_around(): blocks = blocks[(jnp.arange(count) - shift) % count]]
  transfers between devices with their start and end apart: 6 -> 8, of which waited for: 5 -> 6; matrix products, arithmetic and copies ran while one was open for 2% -> 3% of each run, Pallas kernels for 0% -> 0%
where the time goes in v1:
time: 489 us; the launch traced here: 479 us
  waiting for transfers between devices  218 us (45%)
  blocking collectives  84.9 us (17%)
  local copies, waits for them, and re-layouts  78 us (16%)
  matrix products  34.6 us (7%)
  starting transfers between devices  30.7 us (6%)
  other arithmetic  18.2 us (4%)
  between operations  14.4 us (3%)
    all_to_all x1, blocking collectives, local(): lax.all_to_all(padded[slot_table.reshape(experts, 1, capacity)], SP, spli...  69.8 us
    reduce_scatter x1, waiting for transfers between devices, local(): lax.psum_scatter(group_term.reshape(sources, owners, slot_span, width_in)...  55.6 us
    ppermute x2, waiting for transfers between devices, gather_around(): lower.append(lax.ppermute(lower[-1] if lower else x, axis, pairs))  53.8 us
    all_to_all x1, waiting for transfers between devices, local(): lax.all_to_all(summed, SP, split_axis=0, concat_axis=0, tiled=True)  51.1 us
    all_gather x1, waiting for transfers between devices, collected_together(): both, at, found = (lax.all_gather(jnp.concatenate(lines), axis), 0, {})  36.4 us
    all_to_all x1, waiting for transfers between devices, sent_and_summed(): pieces = lax.all_to_all(in_blocks(x, dim, length), axis, 0, 0, tiled=True)  21.3 us
    convert_element_type x2, local copies, waits for them, and re-layouts, local(): group_term.reshape(sources, owners, slot_span, width_in)  19 us
    dot_general x1, matrix products, local(): jnp.dot(hidden_act, expert_down_weight[0], preferred_element_type=jnp.flo...  17.6 us
  transfers between devices with their start and end apart: 8, of which 6 were waited for; matrix products, arithmetic and copies ran while one was open for 3% of the time, Pallas kernels for 0%

profile of v1, /device:TPU:8, one launch (start us, length us, event | category | flops | bytes accessed | tf_op | source)
XLA Modules:
  0.0 479.0 jit_solution(12249007098020033880)
XLA Ops:
  9.8 7.3 %while.21 = (s32[]{:T(128)}, f32[2,128,128]{2,1,0:T(8,128)S(1)}, f32[2,128]{1,0:T(2,128)S(1)}, f32[2]{0:T(128)S(1)}, f32[2,2,256,128]{3,2,0,1:T(8,128)S(1)}, /*i...) while((s32[]{:T(128)}, f32[2,128,128]{2,1,0:T(8,128)S(1)}, ...), condition=%wide.region_6.7_spmd.clone, body=%wide.region_0.6_spmd.clone.sunk | while | flops 102833424 | bytes 3183522 | solution.py:184
  20.7 13.0 %all-gather.4 = f32[4,260,128]{2,1,0:T(8,128)S(1)} all-gather(f32[1,260,128]{2,1,0:T(8,128)S(1)} %maximum_bitcast_fusion.2), channel_id=3, replica_groups=mesh['sp_0'=8,'sp_1'=4,'sp_2'=2,'tp'=4] {'sp_1'}, dimensions={0}, use_global_device_ids=true | all-gather | bytes 665600 | tf_op jit(solution)/shard_map/all_gather | solution.py:49
  36.2 12.4 %all-to-all-start = ((bf16[64,256,32]{1,2,0:T(8,128)(2,1)}), bf16[64,256,32]{1,2,0:T(8,128)(2,1)S(1)}, u32[]{:S(2)}, u32[]{:S(2)}) async-start(bf16[64,256,32]{1,2,0:T(8,128)(2,1)} %broadcast_in_dim.50), calls=%async_computation | async-start | bytes 2097152 | tf_op jit(solution)/shard_map/all_to_all | solution.py:75
  50.1 36.4 %all-gather.8.cloned.1.call-done = f32[8,260,128]{2,1,0:T(8,128)} async-done(((f32[1,260,128]{2,1,0:T(8,128)}), f32[8,260,128]{2,1,0:T(8,128)}) %all-gather.8.cloned.1.call-update) | async-done | bytes 1064976 | tf_op jit(solution)/shard_map/all_gather | solution.py:49
  91.2 4.1 bitcast_convert_fusion
  95.3 4.4 all-to-all-start.1
  103.8 21.3 %all-to-all-done.1 = bf16[4,128,2048]{2,1,0:T(8,128)(2,1)S(1)} async-done(((bf16[4,128,2048]{2,1,0:T(8,128)(2,1)}), bf16[4,128,2048]{2,1,0:T(8,128)(2,1)S(1)}, u32[]{:S(2)}, u32[]{:S(2)}) %all-to-all-start.1) | async-done | bytes 2097184 | tf_op jit(solution)/shard_map/all_to_all | solution.py:96
  130.6 69.8 %all_to_all.20 = bf16[64,1,5,2048]{3,2,1,0:T(8,128)(2,1)S(1)} all-to-all(bf16[64,1,5,2048]{3,2,1,0:T(8,128)(2,1)} %bitcast.698), channel_id=1, replica_groups=mesh['sp_0'=8,'sp_1'=4,'sp_2'=2,'tp'=4] {'sp_0','sp_1','sp_2'}, dimensions={0} | all-to-all | bytes 2621440 | tf_op jit(solution)/shard_map/all_to_all | solution.py:262
  202.9 2.7 collective-permute-start.2
  205.6 27.2 %collective-permute-done = bf16[64,1,5,2048]{3,0,2,1:T(8,128)(2,1)S(1)} collective-permute-done((bf16[64,1,5,2048]{3,0,2,1:T(8,128)(2,1)}, bf16[64,1,5,2048]{3,0,2,1:T(8,128)(2,1)S(1)}, u32[]{:S(2)}, u32[]{:S(2)}) %collective-permute-start) | collective-permute-done | bytes 1310752 | tf_op jit(solution)/shard_map/ppermute | solution.py:26
  235.6 26.6 %collective-permute-done.1 = bf16[64,1,5,2048]{3,0,2,1:T(8,128)(2,1)} collective-permute-done((bf16[64,1,5,2048]{3,0,2,1:T(8,128)(2,1)S(1)}, bf16[64,1,5,2048]{3,0,2,1:T(8,128)(2,1)}, u32[]{:S(2)}, u32[]{:S(2)}) %collective-permute-start.1) | collective-permute-done | bytes 1310752 | tf_op jit(solution)/shard_map/ppermute | solution.py:26
  264.3 4.4 maximum_bitcast_fusion
  268.7 8.0 %gather_fusion.1 = bf16[4,64,5,2048]{3,2,1,0:T(8,128)(2,1)} fusion(bf16[4,64,5,2048]{3,2,1,0:T(8,128)(2,1)} %maximum_bitcast_fusion, s32[1024]{0:T(1024)S(1)} %pad_clamp_fusion.1), kind=kCustom, calls=%fused_computation.1 | custom fusion | bytes 10485776 | tf_op jit(solution)/shard_map/gather | solution.py:31
  276.7 8.3 %copy.133 = bf16[64,4,1,5,2048]{4,3,1,0,2:T(8,128)(2,1)} copy(bf16[64,4,1,5,2048]{4,3,0,1,2:T(8,128)(2,1)} %bitcast.692) | data formatting | bytes 10485760 | tf_op jit(solution)/shard_map/transpose | solution.py:14
  285.0 10.0 %reshape_reshape.10 = bf16[1280,2048]{1,0:T(8,128)(2,1)} reshape(bf16[64,4,1,5,2048]{4,3,1,0,2:T(8,128)(2,1)} %copy.133) | data formatting | bytes 10485760 | tf_op jit(solution)/shard_map/reshape;reshape | solution.py:273
  295.0 10.0 %fusion.36 = f32[1280,896]{1,0:T(8,128)} fusion(bf16[1280,2048]{1,0:T(8,128)(2,1)} %reshape_reshape.10, bf16[1,2048,896]{2,1,0:T(8,128)(2,1)} %param.25), kind=kOutput, calls=%fused_computation.69 | convolution fusion | flops 4697620480 | bytes 13500416 | tf_op jit(solution)/shard_map/dot_general | solution.py:274
  305.0 17.6 %convolution_convert_fusion = bf16[1280,2048]{1,0:T(8,128)(2,1)} fusion(bf16[1,896,2048]{2,1,0:T(8,128)(2,1)} %param.27, f32[1280,896]{1,0:T(8,128)} %fusion.36, bf16[1280,2048]{1,0:T(8,128)(2,1)} %reshape_reshape.10, bf16[1,2048,896]{2,1,0:T(8,128)(2,1)} %param.26), kind=kOutput, calls=%fused_computation.63 | convolution fusion | flops 9404743680 | bytes 22413312 | tf_op jit(solution)/shard_map/dot_general | solution.py:277
  322.6 9.8 %convert_element_type.74 = bf16[64,4,5,2048]{3,2,1,0:T(8,128)(2,1)} reshape(bf16[1280,2048]{1,0:T(8,128)(2,1)} %convolution_convert_fusion) | data formatting | bytes 10485760 | tf_op jit(solution)/shard_map/convert_element_type | solution.py:280
  332.3 9.2 %copy.134 = bf16[64,4,5,2048]{3,0,2,1:T(8,128)(2,1)} copy(bf16[64,4,5,2048]{3,2,1,0:T(8,128)(2,1)} %convert_element_type.74) | data formatting | bytes 10485760 | tf_op jit(solution)/shard_map/convert_element_type | solution.py:280
  341.6 55.6 %reduce-scatter.2.cloned.1.call-done = bf16[64,1,5,2048]{3,0,2,1:T(8,128)(2,1)} async-done(((bf16[64,4,5,2048]{3,0,2,1:T(8,128)(2,1)}), bf16[64,1,5,2048]{3,0,2,1:T(8,128)(2,1)}) %reduce-scatter.2.cloned.1.call-update) | async-done | bytes 1310736 | tf_op jit(solution)/shard_map/reduce_scatter | solution.py:279
  397.2 3.4 copy.135
  400.6 10.6 %all-to-all-start.3 = ((bf16[64,1,5,2048]{3,2,1,0:T(8,128)(2,1)}), bf16[64,1,5,2048]{3,2,1,0:T(8,128)(2,1)S(1)}, u32[]{:S(2)}, u32[]{:S(2)}) async-start(bf16[64,1,5,2048]{3,2,1,0:T(8,128)(2,1)} %copy.135), calls=%async_computation.4 | async-start | bytes 4194304 | tf_op jit(solution)/shard_map/all_to_all | solution.py:285
  411.3 51.1 %all-to-all-done.3 = bf16[64,1,5,2048]{3,2,1,0:T(8,128)(2,1)S(1)} async-done(((bf16[64,1,5,2048]{3,2,1,0:T(8,128)(2,1)}), bf16[64,1,5,2048]{3,2,1,0:T(8,128)(2,1)S(1)}, u32[]{:S(2)}, u32[]{:S(2)}) %all-to-all-start.3) | async-done | bytes 1310752 | tf_op jit(solution)/shard_map/all_to_all | solution.py:285
  467.7 3.2 multiply_reduce_fusion
  (188 shorter events, 45.5 us)
Async XLA Ops:
  6.5 2.8 copy-start.3
  6.5 3.1 copy-start.8
  6.5 3.1 copy-start.7
  6.5 3.2 copy-start.4
  6.5 80.0 %all-gather.8.cloned.1.call-start = ((), (), s32[]{:S(2)}) async-start(), calls=%async_computation.6 | async-start | bytes 1216512 | tf_op jit(solution)/shard_map/all_gather | solution.py:49
  9.7 25.2 %copy-start.5 = (bf16[256,32]{0,1:T(8,128)(2,1)S(1)}, bf16[256,32]{0,1:T(8,128)(2,1)}, u32[]{:S(2)}) copy-start(bf16[256,32]{0,1:T(8,128)(2,1)} %param.23) | copy-start | bytes 49156
  20.4 13.4 %copy-start.12 = (f32[2]{0:T(128)}, f32[2]{0:T(128)S(1)}, u32[]{:S(2)}) copy-start(f32[2]{0:T(128)S(1)} %fusion.339) | copy-start | bytes 28
  33.8 2.3 copy-start.9
  33.8 2.3 copy-start.10
  33.8 53.5 %copy-start.13 = (f32[2]{0:T(128)}, f32[2]{0:T(128)S(1)}, u32[]{:S(2)}) copy-start(f32[2]{0:T(128)S(1)} %fusion.335) | copy-start | bytes 28
  36.2 54.8 %all-to-all-start = ((bf16[64,256,32]{1,2,0:T(8,128)(2,1)}), bf16[64,256,32]{1,2,0:T(8,128)(2,1)S(1)}, u32[]{:S(2)}, u32[]{:S(2)}) async-start(bf16[64,256,32]{1,2,0:T(8,128)(2,1)} %broadcast_in_dim.50), calls=%async_computation | async-start | bytes 2097152 | tf_op jit(solution)/shard_map/all_to_all | solution.py:75
  88.4 2.8 copy-start.14
  95.3 30.1 %copy-start.2 = (bf16[128,2048]{1,0:T(8,128)(2,1)S(1)}, bf16[128,2048]{1,0:T(8,128)(2,1)}, u32[]{:S(2)}) copy-start(bf16[128,2048]{1,0:T(8,128)(2,1)} %param.22) | copy-start | bytes 1572868
  95.3 29.7 %all-to-all-start.1 = ((bf16[4,128,2048]{2,1,0:T(8,128)(2,1)}), bf16[4,128,2048]{2,1,0:T(8,128)(2,1)S(1)}, u32[]{:S(2)}, u32[]{:S(2)}) async-start(bf16[4,128,2048]{2,1,0:T(8,128)(2,1)} %bitcast.706), calls=%async_computation.1 | async-start | bytes 4194304 | tf_op jit(solution)/shard_map/all_to_all | solution.py:96
  99.8 26.0 %copy-start.6 = (f32[2048]{0:T(1024)S(1)}, f32[2048]{0:T(1024)}, u32[]{:S(2)}) copy-start(f32[2048]{0:T(1024)} %param.24) | copy-start | bytes 24580
  99.8 297.4 %reduce-scatter.2.cloned.1.call-start = ((), (), s32[]{:S(2)}) async-start(), calls=%async_computation.5 | async-start | bytes 6553600 | tf_op jit(solution)/shard_map/reduce_scatter | solution.py:279
  125.7 0.8 copy-start
  202.4 30.4 %collective-permute-start = (bf16[64,1,5,2048]{3,0,2,1:T(8,128)(2,1)}, bf16[64,1,5,2048]{3,0,2,1:T(8,128)(2,1)S(1)}, u32[]{:S(2)}, u32[]{:S(2)}) collective-permute-start(bf16[64,1,5,2048]{3,0,2,1:T(8,128)(2,1)} %copy.128), channel_id=1, source_target_pairs={{0,1},{1,2},{2,3},{3,0},{4,5},{5,6},{6,7},{7,4},{8,9},{9,10},{10,1... | collective-permute-start | bytes 3932168 | tf_op jit(solution)/shard_map/ppermute | solution.py:26
  202.9 30.6 %collective-permute-start.2 = (bf16[64,1,5,2048]{3,0,2,1:T(8,128)(2,1)}, bf16[64,1,5,2048]{3,0,2,1:T(8,128)(2,1)}, u32[]{:S(2)}, u32[]{:S(2)}) collective-permute-start(bf16[64,1,5,2048]{3,0,2,1:T(8,128)(2,1)} %copy.128), channel_id=1, source_target_pairs={{1,0},{2,1},{3,2},{0,3},{5,4},{6,5},{7,6},{4,7},{9,8},{10,9},{11,1... | collective-permute-start | bytes 3932168 | tf_op jit(solution)/shard_map/ppermute | solution.py:28
  232.8 29.5 %collective-permute-start.1 = (bf16[64,1,5,2048]{3,0,2,1:T(8,128)(2,1)S(1)}, bf16[64,1,5,2048]{3,0,2,1:T(8,128)(2,1)}, u32[]{:S(2)}, u32[]{:S(2)}) collective-permute-start(bf16[64,1,5,2048]{3,0,2,1:T(8,128)(2,1)S(1)} %collective-permute-done), channel_id=1, source_target_pairs={{0,1},{1,2},{2,3},{3,0},{4,5},{5,6},{6,7},{7,4},{8,9},{9,10},{10,1... | collective-permute-start | bytes 3932168 | tf_op jit(solution)/shard_map/ppermute | solution.py:26
  341.6 69.6 %copy-start.11 = (f32[128,2]{0,1:T(2,128)S(1)}, f32[128,2]{0,1:T(2,128)}, u32[]{:S(2)}) copy-start(f32[128,2]{0,1:T(2,128)} %param.29) | copy-start | bytes 3076
  400.6 61.8 %all-to-all-start.3 = ((bf16[64,1,5,2048]{3,2,1,0:T(8,128)(2,1)}), bf16[64,1,5,2048]{3,2,1,0:T(8,128)(2,1)S(1)}, u32[]{:S(2)}, u32[]{:S(2)}) async-start(bf16[64,1,5,2048]{3,2,1,0:T(8,128)(2,1)} %copy.135), calls=%async_computation.4 | async-start | bytes 4194304 | tf_op jit(solution)/shard_map/all_to_all | solution.py:285
  465.3 5.6 %copy-start.1 = (bf16[128,2048]{1,0:T(8,128)(2,1)S(1)}, bf16[128,2048]{1,0:T(8,128)(2,1)}, u32[]{:S(2)}) copy-start(bf16[128,2048]{1,0:T(8,128)(2,1)} %copy-done) | copy-start | bytes 1572868
Sparse Core Ops, SparseCore 0:
  35.1 51.3 all-gather.7
  341.7 55.4 reduce-scatter.1
